TPU v7x, 256 devices: a whole 4x4x8 slice. The times are simulated.
256 devices in a mesh: ep: 64 (over z, y, core), tp: 4 (over x).
Axes of the slice: x: 4, y: 4, z: 8, core: 2. Of those that a mesh axis runs over, the one named last changes fastest.
Arguments:
- query_rows: bfloat16 [8192, 1024], P('ep', 'tp'), may hold values from -10 to 10
- key_rows: bfloat16 [8192, 1024], P('ep', 'tp'), may hold values from -10 to 10
- value_rows: bfloat16 [8192, 1024], P('ep', 'tp'), may hold values from -6 to 6
- key_bias: bfloat16 [8192, 16], P('ep', 'tp'), may hold values from -24 to 4
- mixer_weight: bfloat16 [1024, 2048], P('tp'), may hold values from -0.1875 to 0.1875
- mixer_gain: float32 [2048], replicated, may hold values from 0.1 to 1.9
- routed_input: bfloat16 [24576, 2048], P(('ep', 'tp')), may hold values from -6 to 6
- entry_gain: float32 [2048], replicated, may hold values from 0.1 to 1.9
- expert_index: int32 [24576, 2], P(('ep', 'tp')), may hold values from 0 to 127, all different within a row; in each aligned block of 96 rows (0 to 95, 96 to 191, ...) at most 2 rows name the same one
- route_weights: float32 [24576, 2], P(('ep', 'tp')), may hold values from 0.1 to 1
- expert_gate: bfloat16 [128, 2048, 1024], P('ep', None, 'tp'), may hold values from -0.125 to 0.125
- expert_up: bfloat16 [128, 2048, 1024], P('ep', None, 'tp'), may hold values from -0.125 to 0.125
- expert_down: bfloat16 [128, 1024, 2048], P('ep', 'tp'), may hold values from -0.1875 to 0.1875
- shared_gate: bfloat16 [2048, 1024], P(None, 'tp'), may hold values from -0.125 to 0.125
- shared_up: bfloat16 [2048, 1024], P(None, 'tp'), may hold values from -0.125 to 0.125
- shared_down: bfloat16 [1024, 2048], P('tp'), may hold values from -0.1875 to 0.1875
- exit_gain: float32 [2048], replicated, may hold values from 0.1 to 1.9
Outputs:
- mixer_out: bfloat16 [8192, 2048], P(('ep', 'tp'))
- expert_out: bfloat16 [24576, 2048], P(('ep', 'tp'))
Inputs may be any that keep to these rules, and one draw needn't show every extreme that they name: `expert_index`: in each aligned block of 96 rows (the rows of one device) no expert is named by more than 2 rows, a bound that some block reaches; each row names 2 different experts.
All inputs are finite; a program needn't handle non-finite values.
Results may differ from a plain program's by a relative error of at most 0.012.
Values may be sent and summed in bfloat16 or wider, within the bound.
No kernel may reach another device: no remote copies, remote signals or barrier semaphores. Data moves between devices by JAX's collectives and lax.ppermute only.
A program may use at most 128 MiB of HBM per device.

v0:
```python
import jax
import jax.numpy as jnp
from jax import lax
from jax.experimental import pallas as pl
from jax.experimental.pallas import tpu as pltpu
from jax.sharding import PartitionSpec as P

EPS = 1e-06
TILE = 128
LANES = 128
TOGETHER = (1, 1, 2, 4)


def root_norm(values, gain_row):
    return values * lax.rsqrt(jnp.mean(values * values, axis=-1, keepdims=True) + EPS) * gain_row


def attention_kernel(slot_ref, query_ref, *refs):
    out_ref, gathered_ref, tri_ref, carry_ref = refs[-4:]
    tiles = query_ref.shape[0] // TILE
    stride = gathered_ref.shape[1]
    keys = 2 * TILE
    slot = slot_ref[0]
    for piece in range(4):
        gathered_ref[slot % 2, 2 * piece : 2 * piece + 2] = refs[piece][...]
        gathered_ref[1 - slot % 2, 2 * piece : 2 * piece + 2] = refs[4 + piece][...]
    row = lax.broadcasted_iota(jnp.int32, (keys, keys), 0)
    col = lax.broadcasted_iota(jnp.int32, (keys, keys), 1)
    tri_ref[...] = (row > col).astype(jnp.float32).astype(jnp.bfloat16)
    out_ref[...] = jnp.zeros(out_ref.shape, jnp.float32)
    carry_ref[...] = jnp.zeros(carry_ref.shape, jnp.float32)

    def pair(place, active, masked_tile):
        group = place // stride
        behind = place % 4 - (slot // 2) % 4
        block = 2 * jnp.where(behind < 0, behind + 4, behind) + (place % stride // 4 + slot // stride) % 2
        start = pl.multiple_of(group * TILE, TILE)
        pair_rows = jnp.concatenate(
            [gathered_ref[side, block, pl.ds(start, TILE), :] for side in (0, 1)], axis=0
        )
        line = lax.broadcasted_iota(jnp.int32, (16, TILE), 0) == group
        base = tiles * TILE
        bias = jnp.concatenate(
            [
                jnp.sum(
                    jnp.where(line, gathered_ref[side, block, base : base + 16, :].astype(jnp.float32), 0.0),
                    axis=0,
                    keepdims=True,
                )
                for side in (0, 1)
            ],
            axis=1,
        )
        rows = slice(active[0] * TILE, tiles * TILE)
        height = (tiles - active[0]) * TILE
        scores = lax.dot_general(
            query_ref[rows, :], pair_rows, (((1,), (1,)), ((), ())), preferred_element_type=jnp.float32
        )
        scores = scores + bias
        log_term = jnp.log(1.0 + jnp.exp(-jnp.abs(scores)))
        fails = jnp.maximum(scores, 0.0) + log_term
        if masked_tile is not None:
            query_at = lax.broadcasted_iota(jnp.int32, (height, keys), 0)
            query_at = jnp.where(query_at < TILE, query_at + (slot % 2) * TILE, keys)
            causal = lax.broadcasted_iota(jnp.int32, (height, keys), 1) < query_at
            fails = jnp.where(causal, fails, 0.0)
        later = jnp.dot(fails.astype(jnp.bfloat16), tri_ref[...], preferred_element_type=jnp.float32)
        carry = carry_ref[rows, 0:1]
        weights = jnp.exp(jnp.minimum(scores, 0.0) - log_term - (later + carry))
        if masked_tile is not None:
            weights = jnp.where(causal, weights, 0.0)
        out_ref[rows, :] += jnp.dot(weights.astype(jnp.bfloat16), pair_rows, preferred_element_type=jnp.float32)
        carry_ref[rows, 0:1] = carry + jnp.sum(fails, axis=1, keepdims=True)

    half = slot // 2
    for segment in reversed(range(tiles)):
        active = range(segment, tiles)
        top = segment * stride + half
        if segment == 0:
            pair(top, active, segment)

            def last(index, _):
                pair(half - 1 - index, active, None)
                return 0

            lax.fori_loop(0, half, last, 0)
            continue
        together = TOGETHER[segment]
        for turn in range(together):
            pair(top - turn, active, segment if turn == 0 else None)

        def turns(index, _, top=top, active=active, together=together):
            for turn in range(together):
                pair(top - (index + 1) * together - turn, active, None)
            return 0

        lax.fori_loop(0, stride // together - 1, turns, 0)


def attend(slot, queries, mine, other):
    tiles = queries.shape[0] // TILE
    return pl.pallas_call(
        attention_kernel,
        grid_spec=pltpu.PrefetchScalarGridSpec(
            num_scalar_prefetch=1,
            grid=(1,),
            in_specs=[
                pl.BlockSpec(queries.shape, lambda i, s: (0, 0)),
            ]
            + [pl.BlockSpec(mine[0].shape, lambda i, s: (0, 0, 0))] * 8,
            out_specs=pl.BlockSpec((tiles * TILE, TILE), lambda i, s: (0, 0)),
            scratch_shapes=[
                pltpu.VMEM((2, 8) + mine[0].shape[1:], jnp.bfloat16),
                pltpu.VMEM((2 * TILE, 2 * TILE), jnp.bfloat16),
                pltpu.VMEM((tiles * TILE, TILE), jnp.float32),
            ],
        ),
        out_shape=jax.ShapeDtypeStruct((tiles * TILE, TILE), jnp.float32),
        name="attend",
    )(slot.reshape(1).astype(jnp.int32), queries, *mine, *other)


def pack_kernel(query_ref, key_ref, value_ref, bias_ref, out_ref):
    f32 = jnp.float32
    rows, heads = bias_ref.shape
    size = query_ref.shape[1] // heads
    bias = jnp.concatenate([bias_ref[...].astype(f32), jnp.zeros((rows, TILE - heads), f32)], axis=1).T
    line = lax.broadcasted_iota(jnp.int32, (16, TILE), 0)
    for head in range(heads):
        lanes = slice(head * size, (head + 1) * size)
        query = query_ref[:, lanes].astype(f32) * size ** (-0.5)
        out_ref[head, :rows, :] = jnp.concatenate([query, jnp.zeros((rows, size), f32)], axis=1).astype(jnp.bfloat16)
        both = jnp.concatenate([key_ref[:, lanes].astype(f32), value_ref[:, lanes].astype(f32)], axis=1)
        out_ref[head, rows : 2 * rows, :] = both.astype(jnp.bfloat16)
        out_ref[head, 2 * rows :, :] = jnp.where(line == 0, bias[head : head + 1, :], 0.0).astype(jnp.bfloat16)


def pack(query_rows, key_rows, value_rows, key_bias):
    rows, heads = key_bias.shape
    return pl.pallas_call(
        pack_kernel,
        out_shape=jax.ShapeDtypeStruct((heads, 2 * rows + 16, TILE), jnp.bfloat16),
        name="pack",
    )(query_rows, key_rows, value_rows, key_bias)


def swiglu(gate, up):
    return gate / (1.0 + jnp.exp(-gate)) * up


def expert_kernel(*refs, sizes):
    count = len(sizes)
    f32, bf16 = jnp.float32, jnp.bfloat16
    rows_in = refs[:count]
    gate_ref, up_ref, down_ref, shared_gate_ref, shared_up_ref, shared_down_ref = refs[count : count + 6]
    rows_out = refs[count + 6 : 2 * count + 6]
    stack_ref = refs[2 * count + 6]
    width = stack_ref.shape[1] - LANES
    start = 0
    for ref, size in zip(rows_in, sizes):
        stack_ref[start : start + size, :] = ref[...]
        start += size
    notes = stack_ref[:, width:].astype(f32)
    weight = notes[:, 0:1] + notes[:, 1:2]
    chosen = notes[:, 2:3]
    rows = stack_ref[:, :width]
    routed = swiglu(
        jnp.dot(rows, gate_ref[0], preferred_element_type=f32), jnp.dot(rows, up_ref[0], preferred_element_type=f32)
    )
    routed = (routed * weight).astype(bf16)
    shared = swiglu(
        jnp.dot(rows, shared_gate_ref[...], preferred_element_type=f32),
        jnp.dot(rows, shared_up_ref[...], preferred_element_type=f32),
    )
    shared = (shared * chosen).astype(bf16)
    tile = shared_down_ref.shape[1] // 8
    for column in range(8):
        lanes = slice(column * tile, (column + 1) * tile)
        result = jnp.dot(routed, down_ref[0, :, lanes], preferred_element_type=f32)
        result = result + jnp.dot(shared, shared_down_ref[:, lanes], preferred_element_type=f32)
        result = result.astype(bf16)
        start = 0
        for ref, size in zip(rows_out, sizes):
            ref[:, lanes] = result[start : start + size]
            start += size


def expert_layer(pieces, expert, shared, which):
    sizes = tuple(piece.shape[0] for piece in pieces)
    full = pieces[0].shape[1]
    width = full - LANES
    return pl.pallas_call(
        lambda *refs: expert_kernel(*refs, sizes=sizes),
        grid=(1,),
        in_specs=[pl.BlockSpec(piece.shape, lambda i: (0, 0)) for piece in pieces]
        + [pl.BlockSpec((1,) + weight.shape[1:], lambda i: (which, 0, 0)) for weight in expert]
        + [pl.BlockSpec(weight.shape, lambda i: (0, 0)) for weight in shared],
        out_specs=[pl.BlockSpec((size, width), lambda i: (0, 0)) for size in sizes],
        out_shape=[jax.ShapeDtypeStruct((size, width), jnp.bfloat16) for size in sizes],
        scratch_shapes=[pltpu.VMEM((sum(sizes), full), jnp.bfloat16)],
        name="expert_layer",
    )(*pieces, *expert, *shared)


def shift(array, by):
    peers = lax.axis_size("tp")
    return lax.ppermute(array, "tp", [(i, (i + by) % peers) for i in range(peers)])


def ring_gather(low, high):
    prev_low = shift(low, 1)
    next_high = shift(high, -1)
    prev_high = shift(high, 1)
    next_low = shift(low, -1)
    far_low = shift(prev_low, 1)
    far_high = shift(next_high, -1)
    return (low, high, prev_low, prev_high, next_low, next_high, far_low, far_high)


def added(first, second):
    return (first.astype(jnp.float32) + second.astype(jnp.float32)).astype(jnp.bfloat16)


def ring_reduce(parts):
    own_low, own_high, prev_low, prev_high, next_low, next_high, far_low, far_high = parts
    back_high = shift(prev_high, -1)
    back_low = shift(next_low, 1)
    from_low = shift(far_low, -1)
    from_high = shift(far_high, 1)
    down_low = shift(added(prev_low, from_low), -1)
    up_high = shift(added(next_high, from_high), 1)
    f32 = jnp.float32
    low = own_low.astype(f32) + down_low.astype(f32) + back_low.astype(f32)
    high = own_high.astype(f32) + back_high.astype(f32) + up_high.astype(f32)
    return (low.astype(jnp.bfloat16), high.astype(jnp.bfloat16))


def after(array, *others):
    return lax.optimization_barrier((array, *others))[0]


def on_device(
    query_rows,
    key_rows,
    value_rows,
    key_bias,
    mixer_weight,
    mixer_gain,
    routed_input,
    entry_gain,
    expert_index,
    route_weights,
    expert_gate,
    expert_up,
    expert_down,
    shared_gate,
    shared_up,
    shared_down,
    exit_gain,
):
    bf16, f32 = jnp.bfloat16, jnp.float32
    shard_rows = query_rows.shape[0]
    head_count = key_bias.shape[1]
    head_size = query_rows.shape[1] // head_count
    ep_size = lax.axis_size("ep")
    ranks = ep_size // head_count
    own_index = lax.axis_index("ep")
    same_rank = [[rank + ranks * head for head in range(head_count)] for rank in range(ranks)]

    row_count = routed_input.shape[0]
    top_count = expert_index.shape[1]
    local_experts = expert_gate.shape[0]
    model_width = routed_input.shape[1]
    expert_count = local_experts * ep_size
    capacity = 3 * row_count * top_count // (2 * expert_count)
    slot_total = expert_count * capacity
    chunk_slots = ep_size * capacity

    normed = root_norm(routed_input.astype(f32), entry_gain).astype(bf16)
    flat_expert = expert_index.reshape(-1)
    places = jnp.arange(row_count * top_count, dtype=jnp.int32)
    earlier = (flat_expert[:, None] == flat_expert[None, :]) & (places[None, :] < places[:, None])
    slot_rank = jnp.sum(earlier.astype(jnp.int32), axis=1)
    slot_index = (
        (flat_expert // local_experts) * local_experts * capacity + (flat_expert % local_experts) * capacity + slot_rank
    )
    selector = (slot_index[None, :] == jnp.arange(slot_total, dtype=jnp.int32)[:, None]).astype(bf16)
    flat_weight = route_weights.reshape(-1)
    weight_high = flat_weight.astype(bf16)
    weight_low = (flat_weight - weight_high.astype(f32)).astype(bf16)
    chosen = (places % top_count == 0).astype(bf16)
    notes = jnp.pad(jnp.stack([weight_high, weight_low, chosen], axis=1), ((0, 0), (0, LANES - 3)))
    any_choice = jnp.sum(selector.reshape(slot_total, row_count, top_count), axis=2)
    outgoing = jnp.concatenate(
        [
            jnp.dot(any_choice, normed, preferred_element_type=f32).astype(bf16),
            jnp.dot(selector, notes, preferred_element_type=f32).astype(bf16),
        ],
        axis=1,
    )

    def exchange(rows):
        return lax.all_to_all(rows, "ep", split_axis=0, concat_axis=0, tiled=True)

    packed = pack(query_rows, key_rows, value_rows, key_bias)
    swapped = lax.all_to_all(packed, "ep", 0, 0, axis_index_groups=same_rank, tiled=True)
    queries = swapped[:, :shard_rows].reshape(head_count * shard_rows, 2 * head_size)
    bias_rows = jnp.pad(swapped[:, 2 * shard_rows], ((0, 16 - head_count), (0, 0)))
    sending = jnp.concatenate(
        [swapped[:, shard_rows : 2 * shard_rows].reshape(head_count * shard_rows, 2 * head_size), bias_rows], axis=0
    )

    def moved(array, target):
        return lax.ppermute(array, "ep", [(i, target(i)) for i in range(ep_size)])

    def around(by):
        return lambda i: i - i % 8 + (i % 8 + 2 * by) % 8

    beside = moved(sending, lambda i: i ^ (ranks // 2))
    near = jnp.stack([sending, beside])
    prev = moved(near, around(1))
    following = moved(near, around(-1))
    across = moved(near, around(2))
    mine = (near, following, across, prev)
    other = tuple(moved(piece, lambda i: i ^ 1) for piece in mine)

    output = attend(own_index % ranks, queries, mine, other)
    outgoing = after(outgoing, sending)
    arrived = exchange(outgoing.reshape(ep_size, local_experts * capacity, model_width + LANES))
    arrived = after(arrived, output)
    low, high = (
        arrived[:, k * capacity : (k + 1) * capacity].reshape(chunk_slots, model_width + LANES)
        for k in range(local_experts)
    )

    expert = (expert_gate, expert_up, expert_down)
    shared = (shared_gate, shared_up, shared_down)
    low, high, prev_low, prev_high, next_low, next_high, far_low, far_high = ring_gather(low, high)
    own_low, prev_low, next_low = expert_layer((low, prev_low, next_low), expert, shared, 0)
    own_high, prev_high, next_high = expert_layer((high, prev_high, next_high), expert, shared, 1)
    (far_low,) = expert_layer((far_low,), expert, shared, 0)
    (far_high,) = expert_layer((far_high,), expert, shared, 1)
    low, high = ring_reduce((own_low, own_high, prev_low, prev_high, next_low, next_high, far_low, far_high))
    rows = jnp.concatenate([part.reshape(ep_size, capacity, model_width) for part in (low, high)], axis=1)
    returned = exchange(rows).reshape(slot_total, model_width)

    per_tile = output[:, head_size:].astype(bf16).reshape(head_count, shard_rows, head_size)
    heads_back = lax.all_to_all(per_tile, "ep", 0, 0, axis_index_groups=same_rank, tiled=True)
    attended = jnp.transpose(heads_back, (1, 0, 2)).reshape(shard_rows, head_count * head_size)
    mixer_term = jnp.dot(attended, mixer_weight, preferred_element_type=f32).astype(bf16)
    mixer_tiles = lax.all_to_all(
        mixer_term.reshape(lax.axis_size("tp"), -1, model_width), "tp", 0, 0, tiled=True
    )
    mixer_sum = jnp.sum(mixer_tiles.astype(f32), axis=0)
    mixer_out = root_norm(mixer_sum, mixer_gain).astype(bf16)

    combined = lax.dot_general(any_choice, returned, (((0,), (0,)), ((), ())), preferred_element_type=f32)
    expert_out = root_norm(combined, exit_gain).astype(bf16)
    return (mixer_out, expert_out)


def solution(mesh):
    in_specs = (
        P("ep", "tp"),
        P("ep", "tp"),
        P("ep", "tp"),
        P("ep", "tp"),
        P("tp", None),
        P(),
        P(("ep", "tp"), None),
        P(),
        P(("ep", "tp"), None),
        P(("ep", "tp"), None),
        P("ep", None, "tp"),
        P("ep", None, "tp"),
        P("ep", "tp", None),
        P(None, "tp"),
        P(None, "tp"),
        P("tp", None),
        P(),
    )
    out_specs = (P(("ep", "tp"), None), P(("ep", "tp"), None))


    return jax.shard_map(on_device, mesh=mesh, in_specs=in_specs, out_specs=out_specs, check_vma=False)
```

profile of v0, /device:TPU:6, one launch (start us, length us, event | category | flops | bytes accessed | tf_op | source)
XLA Modules:
  0.0 239.0 jit_solution(6449800574816960083)
XLA Ops:
  0.7 1.5 copy.65.bias_ref
  2.2 1.8 pack.1
  3.9 8.5 %all-to-all-start = ((bf16[4,272,128]{2,1,0:T(8,128)(2,1)}), bf16[4,272,128]{2,1,0:T(8,128)(2,1)S(1)}, u32[]{:S(2)}, u32[]{:S(2)}) async-start(bf16[4,272,128]{2,1,0:T(8,128)(2,1)} %pack.1), calls=%async_computation | async-start | bytes 557056 | tf_op jit(solution)/shard_map/all_to_all | solution.py:306
  12.4 0.8 copy.68
  13.7 0.8 copy.70
  15.5 1.2 fusion
  16.7 1.2 convolution_convert_fusion
  18.2 5.2 %all-to-all-done = bf16[4,272,128]{2,1,0:T(8,128)(2,1)S(1)} async-done(((bf16[4,272,128]{2,1,0:T(8,128)(2,1)}), bf16[4,272,128]{2,1,0:T(8,128)(2,1)S(1)}, u32[]{:S(2)}, u32[]{:S(2)}) %all-to-all-start) | async-done | bytes 278560 | tf_op jit(solution)/shard_map/all_to_all | solution.py:306
  24.1 1.2 reshape.201
  25.3 6.7 %all-to-all-start.3 = ((bf16[64,4,2176]{2,1,0:T(4,128)(2,1)}), bf16[64,4,2176]{2,1,0:T(4,128)(2,1)S(1)}, u32[]{:S(2)}, u32[]{:S(2)}) async-start(bf16[64,4,2176]{2,1,0:T(4,128)(2,1)} %reshape.201), calls=%async_computation.3 | async-start | bytes 2228224 | tf_op jit(solution)/shard_map/all_to_all | solution.py:303
  32.0 1.7 collective-permute-start
  33.6 27.5 %collective-permute-done = bf16[528,128]{1,0:T(8,128)(2,1)S(1)} collective-permute-done((bf16[528,128]{1,0:T(8,128)(2,1)S(1)}, bf16[528,128]{1,0:T(8,128)(2,1)S(1)}, u32[]{:S(2)}, u32[]{:S(2)}) %collective-permute-start) | collective-permute-done | bytes 135200 | tf_op jit(solution)/shard_map/ppermute | solution.py:314
  61.2 2.8 %collective-permute-start.1 = (bf16[2,528,128]{2,1,0:T(8,128)(2,1)S(1)}, bf16[2,528,128]{2,1,0:T(8,128)(2,1)S(1)}, u32[]{:S(2)}, u32[]{:S(2)}) collective-permute-start(bf16[2,528,128]{2,1,0:T(8,128)(2,1)S(1)} %pad_maximum_fusion.2.refs_0_), channel_id=1, source_target_pairs={{0,24},{4,28},{8,0},{12,4},{16,8},{20,12},{24,16},{28,20},{32,56},... | collective-permute-start | bytes 811016 | tf_op jit(solution)/shard_map/ppermute | solution.py:314
  63.9 0.9 collective-permute-start.2
  64.8 0.9 collective-permute-start.3
  65.7 9.6 %collective-permute-done.1.refs_1_ = bf16[2,528,128]{2,1,0:T(8,128)(2,1)S(1)} collective-permute-done((bf16[2,528,128]{2,1,0:T(8,128)(2,1)S(1)}, bf16[2,528,128]{2,1,0:T(8,128)(2,1)S(1)}, u32[]{:S(2)}, u32[]{:S(2)}) %collective-permute-start.1) | collective-permute-done | bytes 270368 | tf_op jit(solution)/shard_map/ppermute | solution.py:314
  75.7 3.2 %collective-permute-done.3.refs_3_ = bf16[2,528,128]{2,1,0:T(8,128)(2,1)S(1)} collective-permute-done((bf16[2,528,128]{2,1,0:T(8,128)(2,1)S(1)}, bf16[2,528,128]{2,1,0:T(8,128)(2,1)S(1)}, u32[]{:S(2)}, u32[]{:S(2)}) %collective-permute-start.3) | collective-permute-done | bytes 270368 | tf_op jit(solution)/shard_map/ppermute | solution.py:314
  78.9 1.6 collective-permute-done.7.refs_7_
  80.6 13.0 %attend.1 = f32[512,128]{1,0:T(8,128)} custom-call(s32[1]{0:T(128)} %bitcast.slot_ref, bf16[512,128]{1,0:T(8,128)(2,1)} %bitcast.19, bf16[2,528,128]{2,1,0:T(8,128)(2,1)} %copy-done.4, bf16[2,528,128]{2,1,0:T(8,128)(2,1)} %copy-done.13, bf16[2,528,128]{2,1,0:T(8,128)(2,1)} %copy-done.14, bf16[2,528,128]{2,1,0:T(8,128)(2,1)} %copy-done.15, ...), custom_call_target="tpu_custom_call" | custom-call | tf_op jit(solution)/shard_map/attend/pallas_call | solution.py:102
  93.6 0.8 fusion.35
  95.4 1.6 collective-permute-start.15
  97.0 12.4 %collective-permute-done.8.refs_1_ = bf16[128,2176]{1,0:T(8,128)(2,1)} collective-permute-done((bf16[128,2176]{1,0:T(8,128)(2,1)S(1)}, bf16[128,2176]{1,0:T(8,128)(2,1)}, u32[]{:S(2)}, u32[]{:S(2)}) %collective-permute-start.8) | collective-permute-done | bytes 557088 | tf_op jit(solution)/shard_map/ppermute | solution.py:207
  109.5 1.7 collective-permute-start.10
  111.5 0.8 collective-permute-start.9
  112.3 2.4 %collective-permute-start.14 = (bf16[128,2176]{1,0:T(8,128)(2,1)S(1)}, bf16[128,2176]{1,0:T(8,128)(2,1)}, u32[]{:S(2)}, u32[]{:S(2)}) collective-permute-start(bf16[128,2176]{1,0:T(8,128)(2,1)S(1)} %reshape.204.refs_0_), channel_id=1, source_target_pairs={{0,1},{1,2},{2,3},{3,0},{4,5},{5,6},{6,7},{7,4},{8,9},{9,10},{10,1... | collective-permute-start | bytes 1671176 | tf_op jit(solution)/shard_map/ppermute | solution.py:207
  114.8 10.4 %collective-permute-done.10.refs_0_ = bf16[128,2176]{1,0:T(8,128)(2,1)S(1)} collective-permute-done((bf16[128,2176]{1,0:T(8,128)(2,1)}, bf16[128,2176]{1,0:T(8,128)(2,1)S(1)}, u32[]{:S(2)}, u32[]{:S(2)}) %collective-permute-start.10) | collective-permute-done | bytes 557088 | tf_op jit(solution)/shard_map/ppermute | solution.py:207
  125.2 0.8 copy-done.7
  126.0 4.9 %expert_layer.5 = bf16[128,2048]{1,0:T(8,128)(2,1)} custom-call(bf16[128,2176]{1,0:T(8,128)(2,1)} %copy-done.7, bf16[2,2048,256]{2,1,0:T(8,128)(2,1)} %refs_1_.3, bf16[2,2048,256]{2,1,0:T(8,128)(2,1)} %refs_2_.3, bf16[2,256,2048]{2,1,0:T(8,128)(2,1)} %refs_3_.7, bf16[2048,256]{1,0:T(8,128)(2,1)} %refs_4_.7, bf16[2048,256]{1,0:T(8,128)(2,1)} %refs_5_.7, ...), custom_call_target="tpu_custom_call" | custom-call | tf_op jit(solution)/shard_map/expert_layer/pallas_call | solution.py:192
  130.9 1.1 collective-permute-start.11
  132.0 0.8 copy-done.6
  132.8 4.9 %expert_layer.7 = bf16[128,2048]{1,0:T(8,128)(2,1)} custom-call(bf16[128,2176]{1,0:T(8,128)(2,1)} %copy-done.6, bf16[2,2048,256]{2,1,0:T(8,128)(2,1)} %refs_1_.3, bf16[2,2048,256]{2,1,0:T(8,128)(2,1)} %refs_2_.3, bf16[2,256,2048]{2,1,0:T(8,128)(2,1)} %refs_3_.7, bf16[2048,256]{1,0:T(8,128)(2,1)} %refs_4_.7, bf16[2048,256]{1,0:T(8,128)(2,1)} %refs_5_.7, ...), custom_call_target="tpu_custom_call" | custom-call | tf_op jit(solution)/shard_map/expert_layer/pallas_call | solution.py:192
  137.8 2.4 %collective-permute-start.18 = (bf16[128,2048]{1,0:T(8,128)(2,1)}, bf16[128,2048]{1,0:T(8,128)(2,1)S(1)}, u32[]{:S(2)}, u32[]{:S(2)}) collective-permute-start(bf16[128,2048]{1,0:T(8,128)(2,1)} %expert_layer.7), channel_id=1, source_target_pairs={{0,1},{1,2},{2,3},{3,0},{4,5},{5,6},{6,7},{7,4},{8,9},{9,10},{10,1... | collective-permute-start | bytes 1572872 | tf_op jit(solution)/shard_map/ppermute | solution.py:207
  140.9 1.6 copy.67
  142.6 6.2 %all-to-all-start.1 = ((bf16[4,128,64]{1,2,0:T(8,128)(2,1)}), bf16[4,128,64]{1,2,0:T(8,128)(2,1)S(1)}, u32[]{:S(2)}, u32[]{:S(2)}) async-start(bf16[4,128,64]{1,2,0:T(8,128)(2,1)} %copy.67), calls=%async_computation.1 | async-start | bytes 131072 | tf_op jit(solution)/shard_map/all_to_all | solution.py:348
  148.8 7.1 %expert_layer.4 = (bf16[128,2048]{1,0:T(8,128)(2,1)}, bf16[128,2048]{1,0:T(8,128)(2,1)}, bf16[128,2048]{1,0:T(8,128)(2,1)}) custom-call(bf16[128,2176]{1,0:T(8,128)(2,1)} %copy-done.2, bf16[128,2176]{1,0:T(8,128)(2,1)} %collective-permute-done.8.refs_1_, bf16[128,2176]{1,0:T(8,128)(2,1)} %collective-permute-done.9.refs_2_, bf16[2,2048,256]{2,1,0:T(8,128)(2,1)} %refs_1_.3, ...), custom_call_target="tpu_custom_call" | custom-call | tf_op jit(solution)/shard_map/expert_layer/pallas_call | solution.py:192
  155.8 1.7 collective-permute-start.13
  157.5 7.0 %expert_layer.6 = (bf16[128,2048]{1,0:T(8,128)(2,1)}, bf16[128,2048]{1,0:T(8,128)(2,1)}, bf16[128,2048]{1,0:T(8,128)(2,1)}) custom-call(bf16[128,2176]{1,0:T(8,128)(2,1)} %copy-done.1, bf16[128,2176]{1,0:T(8,128)(2,1)} %collective-permute-done.14.refs_1_, bf16[128,2176]{1,0:T(8,128)(2,1)} %collective-permute-done.15.refs_2_, bf16[2,2048,256]{2,1,0:T(8,128)(2,1)} %refs_1_.3, ...), custom_call_target="tpu_custom_call" | custom-call | tf_op jit(solution)/shard_map/expert_layer/pallas_call | solution.py:192
  165.2 1.2 add_convert_fusion.1
  166.4 3.3 %collective-permute-start.19 = (bf16[128,2048]{1,0:T(8,128)(2,1)S(1)}, bf16[128,2048]{1,0:T(8,128)(2,1)}, u32[]{:S(2)}, u32[]{:S(2)}) collective-permute-start(bf16[128,2048]{1,0:T(8,128)(2,1)S(1)} %add_convert_fusion.1), channel_id=1, source_target_pairs={{0,1},{1,2},{2,3},{3,0},{4,5},{5,6},{6,7},{7,4},{8,9},{9,10},{10,1... | collective-permute-start | bytes 1572872 | tf_op jit(solution)/shard_map/ppermute | solution.py:207
  169.7 1.1 convolution_convert_fusion.1
  170.8 5.1 %all-to-all-start.2 = ((bf16[4,32,2048]{2,1,0:T(8,128)(2,1)}), bf16[4,32,2048]{2,1,0:T(8,128)(2,1)S(1)}, u32[]{:S(2)}, u32[]{:S(2)}) async-start(bf16[4,32,2048]{2,1,0:T(8,128)(2,1)} %bitcast.9), calls=%async_computation.2 | async-start | bytes 1048576 | tf_op jit(solution)/shard_map/all_to_all | solution.py:351
  176.0 13.6 %collective-permute-done.12 = bf16[128,2048]{1,0:T(8,128)(2,1)} collective-permute-done((bf16[128,2048]{1,0:T(8,128)(2,1)S(1)}, bf16[128,2048]{1,0:T(8,128)(2,1)}, u32[]{:S(2)}, u32[]{:S(2)}) %collective-permute-start.12) | collective-permute-done | bytes 524320 | tf_op jit(solution)/shard_map/ppermute | solution.py:207
  189.6 1.4 add_convert_fusion.2
  191.1 1.4 add_convert_fusion
  193.2 2.1 pad_maximum_fusion.1
  195.3 13.3 %all-to-all-start.4 = ((bf16[64,4,2048]{2,1,0:T(4,128)(2,1)}), bf16[64,4,2048]{2,1,0:T(4,128)(2,1)S(1)}, u32[]{:S(2)}, u32[]{:S(2)}) async-start(bf16[64,4,2048]{2,1,0:T(4,128)(2,1)} %pad_maximum_fusion.1), calls=%async_computation.4 | async-start | bytes 2097152 | tf_op jit(solution)/shard_map/all_to_all | solution.py:303
  209.5 27.9 %all-to-all-done.4 = bf16[64,4,2048]{2,1,0:T(4,128)(2,1)S(1)} async-done(((bf16[64,4,2048]{2,1,0:T(4,128)(2,1)}), bf16[64,4,2048]{2,1,0:T(4,128)(2,1)S(1)}, u32[]{:S(2)}, u32[]{:S(2)}) %all-to-all-start.4) | async-done | bytes 1048608 | tf_op jit(solution)/shard_map/all_to_all | solution.py:303
  238.1 0.9 multiply_convert_fusion
  (91 shorter events, 8.1 us)
Async XLA Ops:
  0.6 169.1 %copy-start = (bf16[256,2048]{1,0:T(8,128)(2,1)S(1)}, bf16[256,2048]{1,0:T(8,128)(2,1)}, u32[]{:S(2)}) copy-start(bf16[256,2048]{1,0:T(8,128)(2,1)} %param.21) | copy-start | bytes 3145732
  0.6 16.0 %copy-start.3 = (bf16[96,2048]{1,0:T(8,128)(2,1)S(1)}, bf16[96,2048]{1,0:T(8,128)(2,1)}, u32[]{:S(2)}) copy-start(bf16[96,2048]{1,0:T(8,128)(2,1)} %param.23) | copy-start | bytes 1179652
  3.9 19.5 %all-to-all-start = ((bf16[4,272,128]{2,1,0:T(8,128)(2,1)}), bf16[4,272,128]{2,1,0:T(8,128)(2,1)S(1)}, u32[]{:S(2)}, u32[]{:S(2)}) async-start(bf16[4,272,128]{2,1,0:T(8,128)(2,1)} %pack.1), calls=%async_computation | async-start | bytes 557056 | tf_op jit(solution)/shard_map/all_to_all | solution.py:306
  15.5 2.5 %copy-start.11 = (bf16[256,96]{0,1:T(8,128)(2,1)}, bf16[256,96]{0,1:T(8,128)(2,1)S(1)}, u32[]{:S(2)}) copy-start(bf16[256,96]{0,1:T(8,128)(2,1)S(1)} %fusion.14) | copy-start | bytes 147460
  25.3 68.3 %all-to-all-start.3 = ((bf16[64,4,2176]{2,1,0:T(4,128)(2,1)}), bf16[64,4,2176]{2,1,0:T(4,128)(2,1)S(1)}, u32[]{:S(2)}, u32[]{:S(2)}) async-start(bf16[64,4,2176]{2,1,0:T(4,128)(2,1)} %reshape.201), calls=%async_computation.3 | async-start | bytes 2228224 | tf_op jit(solution)/shard_map/all_to_all | solution.py:303
  32.0 29.2 %collective-permute-start = (bf16[528,128]{1,0:T(8,128)(2,1)S(1)}, bf16[528,128]{1,0:T(8,128)(2,1)S(1)}, u32[]{:S(2)}, u32[]{:S(2)}) collective-permute-start(bf16[528,128]{1,0:T(8,128)(2,1)S(1)} %get-tuple-element.23), channel_id=1, source_target_pairs={{0,32},{4,36},{8,40},{12,44},{16,48},{20,52},{24,56},{28,60},{32,0... | collective-permute-start | bytes 405512 | tf_op jit(solution)/shard_map/ppermute | solution.py:314
  61.2 19.4 %copy-start.4 = (bf16[2,528,128]{2,1,0:T(8,128)(2,1)}, bf16[2,528,128]{2,1,0:T(8,128)(2,1)S(1)}, u32[]{:S(2)}) copy-start(bf16[2,528,128]{2,1,0:T(8,128)(2,1)S(1)} %pad_maximum_fusion.2.refs_0_) | copy-start | bytes 811012
  61.2 14.0 %collective-permute-start.1 = (bf16[2,528,128]{2,1,0:T(8,128)(2,1)S(1)}, bf16[2,528,128]{2,1,0:T(8,128)(2,1)S(1)}, u32[]{:S(2)}, u32[]{:S(2)}) collective-permute-start(bf16[2,528,128]{2,1,0:T(8,128)(2,1)S(1)} %pad_maximum_fusion.2.refs_0_), channel_id=1, source_target_pairs={{0,24},{4,28},{8,0},{12,4},{16,8},{20,12},{24,16},{28,20},{32,56},... | collective-permute-start | bytes 811016 | tf_op jit(solution)/shard_map/ppermute | solution.py:314
  63.9 11.3 %collective-permute-start.2 = (bf16[2,528,128]{2,1,0:T(8,128)(2,1)S(1)}, bf16[2,528,128]{2,1,0:T(8,128)(2,1)S(1)}, u32[]{:S(2)}, u32[]{:S(2)}) collective-permute-start(bf16[2,528,128]{2,1,0:T(8,128)(2,1)S(1)} %pad_maximum_fusion.2.refs_0_), channel_id=1, source_target_pairs={{0,16},{4,20},{8,24},{12,28},{16,0},{20,4},{24,8},{28,12},{32,48},... | collective-permute-start | bytes 811016 | tf_op jit(solution)/shard_map/ppermute | solution.py:314
  64.8 14.1 %collective-permute-start.3 = (bf16[2,528,128]{2,1,0:T(8,128)(2,1)S(1)}, bf16[2,528,128]{2,1,0:T(8,128)(2,1)S(1)}, u32[]{:S(2)}, u32[]{:S(2)}) collective-permute-start(bf16[2,528,128]{2,1,0:T(8,128)(2,1)S(1)} %pad_maximum_fusion.2.refs_0_), channel_id=1, source_target_pairs={{0,8},{4,12},{8,16},{12,20},{16,24},{20,28},{24,0},{28,4},{32,40},... | collective-permute-start | bytes 811016 | tf_op jit(solution)/shard_map/ppermute | solution.py:314
  65.7 13.3 %collective-permute-start.4 = (bf16[2,528,128]{2,1,0:T(8,128)(2,1)S(1)}, bf16[2,528,128]{2,1,0:T(8,128)(2,1)S(1)}, u32[]{:S(2)}, u32[]{:S(2)}) collective-permute-start(bf16[2,528,128]{2,1,0:T(8,128)(2,1)S(1)} %pad_maximum_fusion.2.refs_0_), channel_id=1, source_target_pairs={{0,4},{4,0},{8,12},{12,8},{16,20},{20,16},{24,28},{28,24},{32,36},... | collective-permute-start | bytes 811016 | tf_op jit(solution)/shard_map/ppermute | solution.py:314
  75.2 5.4 %copy-start.13 = (bf16[2,528,128]{2,1,0:T(8,128)(2,1)}, bf16[2,528,128]{2,1,0:T(8,128)(2,1)S(1)}, u32[]{:S(2)}) copy-start(bf16[2,528,128]{2,1,0:T(8,128)(2,1)S(1)} %collective-permute-done.1.refs_1_) | copy-start | bytes 811012
  75.2 3.7 %collective-permute-start.5 = (bf16[2,528,128]{2,1,0:T(8,128)(2,1)S(1)}, bf16[2,528,128]{2,1,0:T(8,128)(2,1)}, u32[]{:S(2)}, u32[]{:S(2)}) collective-permute-start(bf16[2,528,128]{2,1,0:T(8,128)(2,1)S(1)} %collective-permute-done.1.refs_1_), channel_id=1, source_target_pairs={{0,4},{4,0},{8,12},{12,8},{16,20},{20,16},{24,28},{28,24},{32,36},... | collective-permute-start | bytes 811016 | tf_op jit(solution)/shard_map/ppermute | solution.py:314
  75.2 5.4 %copy-start.14 = (bf16[2,528,128]{2,1,0:T(8,128)(2,1)}, bf16[2,528,128]{2,1,0:T(8,128)(2,1)S(1)}, u32[]{:S(2)}) copy-start(bf16[2,528,128]{2,1,0:T(8,128)(2,1)S(1)} %collective-permute-done.2.refs_2_) | copy-start | bytes 811012
  75.2 3.7 %collective-permute-start.6 = (bf16[2,528,128]{2,1,0:T(8,128)(2,1)S(1)}, bf16[2,528,128]{2,1,0:T(8,128)(2,1)}, u32[]{:S(2)}, u32[]{:S(2)}) collective-permute-start(bf16[2,528,128]{2,1,0:T(8,128)(2,1)S(1)} %collective-permute-done.2.refs_2_), channel_id=1, source_target_pairs={{0,4},{4,0},{8,12},{12,8},{16,20},{20,16},{24,28},{28,24},{32,36},... | collective-permute-start | bytes 811016 | tf_op jit(solution)/shard_map/ppermute | solution.py:314
  78.9 1.7 copy-start.15
  78.9 1.7 collective-permute-start.7
  78.9 1.7 copy-start.16
  94.6 36.3 %copy-start.2 = (bf16[128,2176]{1,0:T(8,128)(2,1)}, bf16[128,2176]{1,0:T(8,128)(2,1)S(1)}, u32[]{:S(2)}) copy-start(bf16[128,2176]{1,0:T(8,128)(2,1)S(1)} %reshape.202.refs_0_) | copy-start | bytes 1671172
  94.6 14.8 %collective-permute-start.8 = (bf16[128,2176]{1,0:T(8,128)(2,1)S(1)}, bf16[128,2176]{1,0:T(8,128)(2,1)}, u32[]{:S(2)}, u32[]{:S(2)}) collective-permute-start(bf16[128,2176]{1,0:T(8,128)(2,1)S(1)} %reshape.202.refs_0_), channel_id=1, source_target_pairs={{0,1},{1,2},{2,3},{3,0},{4,5},{5,6},{6,7},{7,4},{8,9},{9,10},{10,1... | collective-permute-start | bytes 1671176 | tf_op jit(solution)/shard_map/ppermute | solution.py:207
  95.4 35.5 %copy-start.1 = (bf16[128,2176]{1,0:T(8,128)(2,1)}, bf16[128,2176]{1,0:T(8,128)(2,1)S(1)}, u32[]{:S(2)}) copy-start(bf16[128,2176]{1,0:T(8,128)(2,1)S(1)} %reshape.204.refs_0_) | copy-start | bytes 1671172
  95.4 15.8 %collective-permute-start.15 = (bf16[128,2176]{1,0:T(8,128)(2,1)S(1)}, bf16[128,2176]{1,0:T(8,128)(2,1)}, u32[]{:S(2)}, u32[]{:S(2)}) collective-permute-start(bf16[128,2176]{1,0:T(8,128)(2,1)S(1)} %reshape.204.refs_0_), channel_id=1, source_target_pairs={{0,3},{1,0},{2,1},{3,2},{4,7},{5,4},{6,5},{7,6},{8,11},{9,8},{10,9... | collective-permute-start | bytes 1671176 | tf_op jit(solution)/shard_map/ppermute | solution.py:207
  109.5 15.7 %collective-permute-start.10 = (bf16[128,2176]{1,0:T(8,128)(2,1)}, bf16[128,2176]{1,0:T(8,128)(2,1)S(1)}, u32[]{:S(2)}, u32[]{:S(2)}) collective-permute-start(bf16[128,2176]{1,0:T(8,128)(2,1)} %collective-permute-done.8.refs_1_), channel_id=1, source_target_pairs={{0,1},{1,2},{2,3},{3,0},{4,5},{5,6},{6,7},{7,4},{8,9},{9,10},{10,1... | collective-permute-start | bytes 1671176 | tf_op jit(solution)/shard_map/ppermute | solution.py:207
  111.2 20.9 %collective-permute-start.17 = (bf16[128,2176]{1,0:T(8,128)(2,1)}, bf16[128,2176]{1,0:T(8,128)(2,1)S(1)}, u32[]{:S(2)}, u32[]{:S(2)}) collective-permute-start(bf16[128,2176]{1,0:T(8,128)(2,1)} %collective-permute-done.15.refs_2_), channel_id=1, source_target_pairs={{0,3},{1,0},{2,1},{3,2},{4,7},{5,4},{6,5},{7,6},{8,11},{9,8},{10,9... | collective-permute-start | bytes 1671176 | tf_op jit(solution)/shard_map/ppermute | solution.py:207
  111.5 37.3 %collective-permute-start.9 = (bf16[128,2176]{1,0:T(8,128)(2,1)S(1)}, bf16[128,2176]{1,0:T(8,128)(2,1)}, u32[]{:S(2)}, u32[]{:S(2)}) collective-permute-start(bf16[128,2176]{1,0:T(8,128)(2,1)S(1)} %reshape.202.refs_0_), channel_id=1, source_target_pairs={{0,3},{1,0},{2,1},{3,2},{4,7},{5,4},{6,5},{7,6},{8,11},{9,8},{10,9... | collective-permute-start | bytes 1671176 | tf_op jit(solution)/shard_map/ppermute | solution.py:207
  112.3 45.2 %collective-permute-start.14 = (bf16[128,2176]{1,0:T(8,128)(2,1)S(1)}, bf16[128,2176]{1,0:T(8,128)(2,1)}, u32[]{:S(2)}, u32[]{:S(2)}) collective-permute-start(bf16[128,2176]{1,0:T(8,128)(2,1)S(1)} %reshape.204.refs_0_), channel_id=1, source_target_pairs={{0,1},{1,2},{2,3},{3,0},{4,5},{5,6},{6,7},{7,4},{8,9},{9,10},{10,1... | collective-permute-start | bytes 1671176 | tf_op jit(solution)/shard_map/ppermute | solution.py:207
  125.2 0.8 copy-start.7
  130.9 9.3 %copy-start.5 = (f32[512,128]{1,0:T(8,128)S(1)}, f32[512,128]{1,0:T(8,128)}, u32[]{:S(2)}) copy-start(f32[512,128]{1,0:T(8,128)} %attend.1) | copy-start | bytes 786436
  130.9 34.0 %collective-permute-start.11 = (bf16[128,2048]{1,0:T(8,128)(2,1)}, bf16[128,2048]{1,0:T(8,128)(2,1)S(1)}, u32[]{:S(2)}, u32[]{:S(2)}) collective-permute-start(bf16[128,2048]{1,0:T(8,128)(2,1)} %expert_layer.5), channel_id=1, source_target_pairs={{0,3},{1,0},{2,1},{3,2},{4,7},{5,4},{6,5},{7,6},{8,11},{9,8},{10,9... | collective-permute-start | bytes 1572872 | tf_op jit(solution)/shard_map/ppermute | solution.py:207
  132.0 0.8 copy-start.6
  137.8 27.4 %collective-permute-start.18 = (bf16[128,2048]{1,0:T(8,128)(2,1)}, bf16[128,2048]{1,0:T(8,128)(2,1)S(1)}, u32[]{:S(2)}, u32[]{:S(2)}) collective-permute-start(bf16[128,2048]{1,0:T(8,128)(2,1)} %expert_layer.7), channel_id=1, source_target_pairs={{0,1},{1,2},{2,3},{3,0},{4,5},{5,6},{6,7},{7,4},{8,9},{9,10},{10,1... | collective-permute-start | bytes 1572872 | tf_op jit(solution)/shard_map/ppermute | solution.py:207
  142.6 27.1 %all-to-all-start.1 = ((bf16[4,128,64]{1,2,0:T(8,128)(2,1)}), bf16[4,128,64]{1,2,0:T(8,128)(2,1)S(1)}, u32[]{:S(2)}, u32[]{:S(2)}) async-start(bf16[4,128,64]{1,2,0:T(8,128)(2,1)} %copy.67), calls=%async_computation.1 | async-start | bytes 131072 | tf_op jit(solution)/shard_map/all_to_all | solution.py:348
  155.8 9.1 %copy-start.8 = (bf16[128,2048]{1,0:T(8,128)(2,1)S(1)}, bf16[128,2048]{1,0:T(8,128)(2,1)}, u32[]{:S(2)}) copy-start(bf16[128,2048]{1,0:T(8,128)(2,1)} %get-tuple-element.13) | copy-start | bytes 1572868
  155.8 20.1 %collective-permute-start.13 = (bf16[128,2048]{1,0:T(8,128)(2,1)}, bf16[128,2048]{1,0:T(8,128)(2,1)}, u32[]{:S(2)}, u32[]{:S(2)}) collective-permute-start(bf16[128,2048]{1,0:T(8,128)(2,1)} %get-tuple-element.14), channel_id=1, source_target_pairs={{0,1},{1,2},{2,3},{3,0},{4,5},{5,6},{6,7},{7,4},{8,9},{9,10},{10,1... | collective-permute-start | bytes 1572872 | tf_op jit(solution)/shard_map/ppermute | solution.py:207
  164.6 26.5 %collective-permute-start.16 = (bf16[128,2048]{1,0:T(8,128)(2,1)}, bf16[128,2048]{1,0:T(8,128)(2,1)}, u32[]{:S(2)}, u32[]{:S(2)}) collective-permute-start(bf16[128,2048]{1,0:T(8,128)(2,1)} %get-tuple-element.16), channel_id=1, source_target_pairs={{0,3},{1,0},{2,1},{3,2},{4,7},{5,4},{6,5},{7,6},{8,11},{9,8},{10,9... | collective-permute-start | bytes 1572872 | tf_op jit(solution)/shard_map/ppermute | solution.py:207
  165.1 24.5 %collective-permute-start.12 = (bf16[128,2048]{1,0:T(8,128)(2,1)S(1)}, bf16[128,2048]{1,0:T(8,128)(2,1)}, u32[]{:S(2)}, u32[]{:S(2)}) collective-permute-start(bf16[128,2048]{1,0:T(8,128)(2,1)S(1)} %add_convert_fusion.3), channel_id=1, source_target_pairs={{0,3},{1,0},{2,1},{3,2},{4,7},{5,4},{6,5},{7,6},{8,11},{9,8},{10,9... | collective-permute-start | bytes 1572872 | tf_op jit(solution)/shard_map/ppermute | solution.py:207
  165.2 24.4 %copy-start.9 = (bf16[128,2048]{1,0:T(8,128)(2,1)S(1)}, bf16[128,2048]{1,0:T(8,128)(2,1)}, u32[]{:S(2)}) copy-start(bf16[128,2048]{1,0:T(8,128)(2,1)} %get-tuple-element.12) | copy-start | bytes 1572868
  166.4 24.7 %collective-permute-start.19 = (bf16[128,2048]{1,0:T(8,128)(2,1)S(1)}, bf16[128,2048]{1,0:T(8,128)(2,1)}, u32[]{:S(2)}, u32[]{:S(2)}) collective-permute-start(bf16[128,2048]{1,0:T(8,128)(2,1)S(1)} %add_convert_fusion.1), channel_id=1, source_target_pairs={{0,1},{1,2},{2,3},{3,0},{4,5},{5,6},{6,7},{7,4},{8,9},{9,10},{10,1... | collective-permute-start | bytes 1572872 | tf_op jit(solution)/shard_map/ppermute | solution.py:207
  170.8 24.4 %all-to-all-start.2 = ((bf16[4,32,2048]{2,1,0:T(8,128)(2,1)}), bf16[4,32,2048]{2,1,0:T(8,128)(2,1)S(1)}, u32[]{:S(2)}, u32[]{:S(2)}) async-start(bf16[4,32,2048]{2,1,0:T(8,128)(2,1)} %bitcast.9), calls=%async_computation.2 | async-start | bytes 1048576 | tf_op jit(solution)/shard_map/all_to_all | solution.py:351
  175.9 15.1 %copy-start.10 = (bf16[128,2048]{1,0:T(8,128)(2,1)S(1)}, bf16[128,2048]{1,0:T(8,128)(2,1)}, u32[]{:S(2)}) copy-start(bf16[128,2048]{1,0:T(8,128)(2,1)} %get-tuple-element.15) | copy-start | bytes 1572868
  195.3 13.5 %copy-start.18 = (f32[2048]{0:T(1024)S(1)}, f32[2048]{0:T(1024)}, u32[]{:S(2)}) copy-start(f32[2048]{0:T(1024)} %param.22) | copy-start | bytes 24580
  195.3 42.1 %all-to-all-start.4 = ((bf16[64,4,2048]{2,1,0:T(4,128)(2,1)}), bf16[64,4,2048]{2,1,0:T(4,128)(2,1)S(1)}, u32[]{:S(2)}, u32[]{:S(2)}) async-start(bf16[64,4,2048]{2,1,0:T(4,128)(2,1)} %pad_maximum_fusion.1), calls=%async_computation.4 | async-start | bytes 2097152 | tf_op jit(solution)/shard_map/all_to_all | solution.py:303
  208.5 29.1 %copy-start.12 = (bf16[256,96]{0,1:T(8,128)(2,1)S(1)}, bf16[256,96]{0,1:T(8,128)(2,1)}, u32[]{:S(2)}) copy-start(bf16[256,96]{0,1:T(8,128)(2,1)} %copy-done.11) | copy-start | bytes 147460
  208.8 29.3 %copy-start.17 = (f32[2048]{0:T(1024)S(1)}, f32[2048]{0:T(1024)}, u32[]{:S(2)}) copy-start(f32[2048]{0:T(1024)} %param.33) | copy-start | bytes 24580
where the time goes:
time: 240 us; the launch traced here: 239 us
  waiting for transfers between devices  111 us (46%)
  starting transfers between devices  62.8 us (26%)
  Pallas kernels  38.7 us (16%)
  local copies, waits for them, and re-layouts  11.6 us (5%)
  other arithmetic  10.5 us (4%)
  matrix products  2.92 us (1%)
    ppermute x8, waiting for transfers between devices, moved(): return lax.ppermute(array, 'ep', [(i, target(i)) for i in range(ep_size)])  41.8 us
    ppermute x12, waiting for transfers between devices, shift(): lax.ppermute(array, 'tp', [(i, (i + by) % peers) for i in range(peers)])  36.6 us
    all_to_all x2, waiting for transfers between devices, exchange(): return lax.all_to_all(rows, 'ep', split_axis=0, concat_axis=0, tiled=True)  27.9 us
    pallas_call x4, Pallas kernels, expert_layer(): pl.pallas_call(lambda *refs: expert_kernel(*refs, sizes=sizes), grid=(1,)...  24 us
    all_to_all x2, starting transfers between devices, exchange(): return lax.all_to_all(rows, 'ep', split_axis=0, concat_axis=0, tiled=True)  19.9 us
    ppermute x12, starting transfers between devices, shift(): lax.ppermute(array, 'tp', [(i, (i + by) % peers) for i in range(peers)])  16.4 us
    pallas_call x1, Pallas kernels, attend(): pl.pallas_call(attention_kernel, grid_spec=pltpu.PrefetchScalarGridSpec(n...  13 us
    all_to_all x1, starting transfers between devices, on_device(): lax.all_to_all(packed, 'ep', 0, 0, axis_index_groups=same_rank, tiled=True)  8.46 us
  transfers between devices with their start and end apart: 25, of which 9 were waited for; matrix products, arithmetic and copies ran while one was open for 7% of the time, Pallas kernels for 15%

commit v1 on v0

--- a/solution.py
+++ b/solution.py
@@ -122,9 +122,9 @@
 
 def pack_kernel(query_ref, key_ref, value_ref, bias_ref, out_ref):
     f32 = jnp.float32
-    rows, heads = bias_ref.shape
+    heads, rows = bias_ref.shape
     size = query_ref.shape[1] // heads
-    bias = jnp.concatenate([bias_ref[...].astype(f32), jnp.zeros((rows, TILE - heads), f32)], axis=1).T
+    bias = bias_ref[...].astype(f32)
     line = lax.broadcasted_iota(jnp.int32, (16, TILE), 0)
     for head in range(heads):
         lanes = slice(head * size, (head + 1) * size)
@@ -141,7 +141,7 @@
         pack_kernel,
         out_shape=jax.ShapeDtypeStruct((heads, 2 * rows + 16, TILE), jnp.bfloat16),
         name="pack",
-    )(query_rows, key_rows, value_rows, key_bias)
+    )(query_rows, key_rows, value_rows, jnp.transpose(key_bias))
 
 
 def swiglu(gate, up):
@@ -277,7 +277,7 @@
     chunk_slots = ep_size * capacity
 
     normed = root_norm(routed_input.astype(f32), entry_gain).astype(bf16)
-    flat_expert = expert_index.reshape(-1)
+    flat_expert = jnp.transpose(expert_index).reshape(-1)
     places = jnp.arange(row_count * top_count, dtype=jnp.int32)
     earlier = (flat_expert[:, None] == flat_expert[None, :]) & (places[None, :] < places[:, None])
     slot_rank = jnp.sum(earlier.astype(jnp.int32), axis=1)
@@ -285,12 +285,12 @@
         (flat_expert // local_experts) * local_experts * capacity + (flat_expert % local_experts) * capacity + slot_rank
     )
     selector = (slot_index[None, :] == jnp.arange(slot_total, dtype=jnp.int32)[:, None]).astype(bf16)
-    flat_weight = route_weights.reshape(-1)
+    flat_weight = jnp.transpose(route_weights).reshape(-1)
     weight_high = flat_weight.astype(bf16)
     weight_low = (flat_weight - weight_high.astype(f32)).astype(bf16)
-    chosen = (places % top_count == 0).astype(bf16)
+    chosen = (places < row_count).astype(bf16)
     notes = jnp.pad(jnp.stack([weight_high, weight_low, chosen], axis=1), ((0, 0), (0, LANES - 3)))
-    any_choice = jnp.sum(selector.reshape(slot_total, row_count, top_count), axis=2)
+    any_choice = jnp.sum(selector.reshape(slot_total, top_count, row_count), axis=1)
     outgoing = jnp.concatenate(
         [
             jnp.dot(any_choice, normed, preferred_element_type=f32).astype(bf16),

time: 240 us -> 238 us (level)
    unnamed x42 -> x37, local copies, waits for them, and re-layouts: 4.76 us -> 1.69 us
  transfers between devices with their start and end apart: 25 -> 25, of which waited for: 9 -> 9; matrix products, arithmetic and copies ran while one was open for 7% -> 7% of each run, Pallas kernels for 15% -> 16%
where the time goes in v1:
time: 238 us; the launch traced here: 237 us
  waiting for transfers between devices  112 us (47%)
  starting transfers between devices  62.5 us (26%)
  Pallas kernels  39 us (16%)
  other arithmetic  10.5 us (4%)
  local copies, waits for them, and re-layouts  9.64 us (4%)
  matrix products  3.21 us (1%)
    ppermute x8, waiting for transfers between devices, moved(): return lax.ppermute(array, 'ep', [(i, target(i)) for i in range(ep_size)])  41.8 us
    ppermute x12, waiting for transfers between devices, shift(): lax.ppermute(array, 'tp', [(i, (i + by) % peers) for i in range(peers)])  36.5 us
    all_to_all x2, waiting for transfers between devices, exchange(): return lax.all_to_all(rows, 'ep', split_axis=0, concat_axis=0, tiled=True)  27.9 us
    pallas_call x4, Pallas kernels, expert_layer(): pl.pallas_call(lambda *refs: expert_kernel(*refs, sizes=sizes), grid=(1,)...  24 us
    all_to_all x2, starting transfers between devices, exchange(): return lax.all_to_all(rows, 'ep', split_axis=0, concat_axis=0, tiled=True)  19.9 us
    ppermute x12, starting transfers between devices, shift(): lax.ppermute(array, 'tp', [(i, (i + by) % peers) for i in range(peers)])  16.2 us
    pallas_call x1, Pallas kernels, attend(): pl.pallas_call(attention_kernel, grid_spec=pltpu.PrefetchScalarGridSpec(n...  13.2 us
    all_to_all x1, starting transfers between devices, on_device(): lax.all_to_all(packed, 'ep', 0, 0, axis_index_groups=same_rank, tiled=True)  8.46 us
  transfers between devices with their start and end apart: 25, of which 9 were waited for; matrix products, arithmetic and copies ran while one was open for 7% of the time, Pallas kernels for 16%

profile of v1, /device:TPU:6, one launch (start us, length us, event | category | flops | bytes accessed | tf_op | source)
XLA Modules:
  0.0 237.5 jit_solution(8618365884057339907)
XLA Ops:
  0.6 1.8 pack.1
  2.5 8.5 %all-to-all-start = ((bf16[4,272,128]{2,1,0:T(8,128)(2,1)}), bf16[4,272,128]{2,1,0:T(8,128)(2,1)S(1)}, u32[]{:S(2)}, u32[]{:S(2)}) async-start(bf16[4,272,128]{2,1,0:T(8,128)(2,1)} %pack.1), calls=%async_computation | async-start | bytes 557056 | tf_op jit(solution)/shard_map/all_to_all | solution.py:306
  10.9 0.8 eq.39
  12.0 0.8 reshape.182
  13.6 1.2 fusion
  14.8 1.5 convolution_convert_fusion
  16.6 5.4 %all-to-all-done = bf16[4,272,128]{2,1,0:T(8,128)(2,1)S(1)} async-done(((bf16[4,272,128]{2,1,0:T(8,128)(2,1)}), bf16[4,272,128]{2,1,0:T(8,128)(2,1)S(1)}, u32[]{:S(2)}, u32[]{:S(2)}) %all-to-all-start) | async-done | bytes 278560 | tf_op jit(solution)/shard_map/all_to_all | solution.py:306
  22.7 1.2 reshape.183
  23.8 6.7 %all-to-all-start.3 = ((bf16[64,4,2176]{2,1,0:T(4,128)(2,1)}), bf16[64,4,2176]{2,1,0:T(4,128)(2,1)S(1)}, u32[]{:S(2)}, u32[]{:S(2)}) async-start(bf16[64,4,2176]{2,1,0:T(4,128)(2,1)} %reshape.183), calls=%async_computation.3 | async-start | bytes 2228224 | tf_op jit(solution)/shard_map/all_to_all | solution.py:303
  30.5 1.7 collective-permute-start
  32.2 27.5 %collective-permute-done = bf16[528,128]{1,0:T(8,128)(2,1)S(1)} collective-permute-done((bf16[528,128]{1,0:T(8,128)(2,1)S(1)}, bf16[528,128]{1,0:T(8,128)(2,1)S(1)}, u32[]{:S(2)}, u32[]{:S(2)}) %collective-permute-start) | collective-permute-done | bytes 135200 | tf_op jit(solution)/shard_map/ppermute | solution.py:314
  59.7 2.8 %collective-permute-start.1 = (bf16[2,528,128]{2,1,0:T(8,128)(2,1)S(1)}, bf16[2,528,128]{2,1,0:T(8,128)(2,1)S(1)}, u32[]{:S(2)}, u32[]{:S(2)}) collective-permute-start(bf16[2,528,128]{2,1,0:T(8,128)(2,1)S(1)} %pad_maximum_fusion.2.refs_0_), channel_id=1, source_target_pairs={{0,24},{4,28},{8,0},{12,4},{16,8},{20,12},{24,16},{28,20},{32,56},... | collective-permute-start | bytes 811016 | tf_op jit(solution)/shard_map/ppermute | solution.py:314
  62.5 0.9 collective-permute-start.2
  63.3 0.9 collective-permute-start.3
  64.2 9.6 %collective-permute-done.1.refs_1_ = bf16[2,528,128]{2,1,0:T(8,128)(2,1)S(1)} collective-permute-done((bf16[2,528,128]{2,1,0:T(8,128)(2,1)S(1)}, bf16[2,528,128]{2,1,0:T(8,128)(2,1)S(1)}, u32[]{:S(2)}, u32[]{:S(2)}) %collective-permute-start.1) | collective-permute-done | bytes 270368 | tf_op jit(solution)/shard_map/ppermute | solution.py:314
  74.3 3.2 %collective-permute-done.3.refs_3_ = bf16[2,528,128]{2,1,0:T(8,128)(2,1)S(1)} collective-permute-done((bf16[2,528,128]{2,1,0:T(8,128)(2,1)S(1)}, bf16[2,528,128]{2,1,0:T(8,128)(2,1)S(1)}, u32[]{:S(2)}, u32[]{:S(2)}) %collective-permute-start.3) | collective-permute-done | bytes 270368 | tf_op jit(solution)/shard_map/ppermute | solution.py:314
  77.5 1.6 collective-permute-done.7.refs_7_
  79.1 13.2 %attend.1 = f32[512,128]{1,0:T(8,128)} custom-call(s32[1]{0:T(128)} %bitcast.slot_ref, bf16[512,128]{1,0:T(8,128)(2,1)} %bitcast.23, bf16[2,528,128]{2,1,0:T(8,128)(2,1)} %copy-done.3, bf16[2,528,128]{2,1,0:T(8,128)(2,1)} %copy-done.12, bf16[2,528,128]{2,1,0:T(8,128)(2,1)} %copy-done.13, bf16[2,528,128]{2,1,0:T(8,128)(2,1)} %copy-done.14, ...), custom_call_target="tpu_custom_call" | custom-call | tf_op jit(solution)/shard_map/attend/pallas_call | solution.py:102
  92.3 0.8 fusion.35
  94.1 1.6 collective-permute-start.15
  95.7 12.4 %collective-permute-done.8.refs_1_ = bf16[128,2176]{1,0:T(8,128)(2,1)} collective-permute-done((bf16[128,2176]{1,0:T(8,128)(2,1)S(1)}, bf16[128,2176]{1,0:T(8,128)(2,1)}, u32[]{:S(2)}, u32[]{:S(2)}) %collective-permute-start.8) | collective-permute-done | bytes 557088 | tf_op jit(solution)/shard_map/ppermute | solution.py:207
  108.2 1.7 collective-permute-start.10
  110.2 0.8 collective-permute-start.9
  111.0 2.4 %collective-permute-start.14 = (bf16[128,2176]{1,0:T(8,128)(2,1)S(1)}, bf16[128,2176]{1,0:T(8,128)(2,1)}, u32[]{:S(2)}, u32[]{:S(2)}) collective-permute-start(bf16[128,2176]{1,0:T(8,128)(2,1)S(1)} %reshape.186.refs_0_), channel_id=1, source_target_pairs={{0,1},{1,2},{2,3},{3,0},{4,5},{5,6},{6,7},{7,4},{8,9},{9,10},{10,1... | collective-permute-start | bytes 1671176 | tf_op jit(solution)/shard_map/ppermute | solution.py:207
  113.4 10.4 %collective-permute-done.10.refs_0_ = bf16[128,2176]{1,0:T(8,128)(2,1)S(1)} collective-permute-done((bf16[128,2176]{1,0:T(8,128)(2,1)}, bf16[128,2176]{1,0:T(8,128)(2,1)S(1)}, u32[]{:S(2)}, u32[]{:S(2)}) %collective-permute-start.10) | collective-permute-done | bytes 557088 | tf_op jit(solution)/shard_map/ppermute | solution.py:207
  123.9 0.8 copy-done.6
  124.7 5.0 %expert_layer.5 = bf16[128,2048]{1,0:T(8,128)(2,1)} custom-call(bf16[128,2176]{1,0:T(8,128)(2,1)} %copy-done.6, bf16[2,2048,256]{2,1,0:T(8,128)(2,1)} %refs_1_.3, bf16[2,2048,256]{2,1,0:T(8,128)(2,1)} %refs_2_.3, bf16[2,256,2048]{2,1,0:T(8,128)(2,1)} %refs_3_.7, bf16[2048,256]{1,0:T(8,128)(2,1)} %refs_4_.7, bf16[2048,256]{1,0:T(8,128)(2,1)} %refs_5_.7, ...), custom_call_target="tpu_custom_call" | custom-call | tf_op jit(solution)/shard_map/expert_layer/pallas_call | solution.py:192
  129.6 0.9 collective-permute-start.11
  130.5 0.8 copy-done.5
  131.3 4.9 %expert_layer.7 = bf16[128,2048]{1,0:T(8,128)(2,1)} custom-call(bf16[128,2176]{1,0:T(8,128)(2,1)} %copy-done.5, bf16[2,2048,256]{2,1,0:T(8,128)(2,1)} %refs_1_.3, bf16[2,2048,256]{2,1,0:T(8,128)(2,1)} %refs_2_.3, bf16[2,256,2048]{2,1,0:T(8,128)(2,1)} %refs_3_.7, bf16[2048,256]{1,0:T(8,128)(2,1)} %refs_4_.7, bf16[2048,256]{1,0:T(8,128)(2,1)} %refs_5_.7, ...), custom_call_target="tpu_custom_call" | custom-call | tf_op jit(solution)/shard_map/expert_layer/pallas_call | solution.py:192
  136.2 2.4 %collective-permute-start.18 = (bf16[128,2048]{1,0:T(8,128)(2,1)}, bf16[128,2048]{1,0:T(8,128)(2,1)S(1)}, u32[]{:S(2)}, u32[]{:S(2)}) collective-permute-start(bf16[128,2048]{1,0:T(8,128)(2,1)} %expert_layer.7), channel_id=1, source_target_pairs={{0,1},{1,2},{2,3},{3,0},{4,5},{5,6},{6,7},{7,4},{8,9},{9,10},{10,1... | collective-permute-start | bytes 1572872 | tf_op jit(solution)/shard_map/ppermute | solution.py:207
  138.7 0.8 slice.30
  139.4 1.6 copy.30
  141.0 6.2 %all-to-all-start.1 = ((bf16[4,128,64]{1,2,0:T(8,128)(2,1)}), bf16[4,128,64]{1,2,0:T(8,128)(2,1)S(1)}, u32[]{:S(2)}, u32[]{:S(2)}) async-start(bf16[4,128,64]{1,2,0:T(8,128)(2,1)} %copy.30), calls=%async_computation.1 | async-start | bytes 131072 | tf_op jit(solution)/shard_map/all_to_all | solution.py:348
  147.3 7.1 %expert_layer.4 = (bf16[128,2048]{1,0:T(8,128)(2,1)}, bf16[128,2048]{1,0:T(8,128)(2,1)}, bf16[128,2048]{1,0:T(8,128)(2,1)}) custom-call(bf16[128,2176]{1,0:T(8,128)(2,1)} %copy-done.2, bf16[128,2176]{1,0:T(8,128)(2,1)} %collective-permute-done.8.refs_1_, bf16[128,2176]{1,0:T(8,128)(2,1)} %collective-permute-done.9.refs_2_, bf16[2,2048,256]{2,1,0:T(8,128)(2,1)} %refs_1_.3, ...), custom_call_target="tpu_custom_call" | custom-call | tf_op jit(solution)/shard_map/expert_layer/pallas_call | solution.py:192
  154.3 1.7 collective-permute-start.13
  156.0 7.1 %expert_layer.6 = (bf16[128,2048]{1,0:T(8,128)(2,1)}, bf16[128,2048]{1,0:T(8,128)(2,1)}, bf16[128,2048]{1,0:T(8,128)(2,1)}) custom-call(bf16[128,2176]{1,0:T(8,128)(2,1)} %copy-done.1, bf16[128,2176]{1,0:T(8,128)(2,1)} %collective-permute-done.14.refs_1_, bf16[128,2176]{1,0:T(8,128)(2,1)} %collective-permute-done.15.refs_2_, bf16[2,2048,256]{2,1,0:T(8,128)(2,1)} %refs_1_.3, ...), custom_call_target="tpu_custom_call" | custom-call | tf_op jit(solution)/shard_map/expert_layer/pallas_call | solution.py:192
  163.7 1.2 add_convert_fusion.1
  164.9 3.3 %collective-permute-start.19 = (bf16[128,2048]{1,0:T(8,128)(2,1)S(1)}, bf16[128,2048]{1,0:T(8,128)(2,1)}, u32[]{:S(2)}, u32[]{:S(2)}) collective-permute-start(bf16[128,2048]{1,0:T(8,128)(2,1)S(1)} %add_convert_fusion.1), channel_id=1, source_target_pairs={{0,1},{1,2},{2,3},{3,0},{4,5},{5,6},{6,7},{7,4},{8,9},{9,10},{10,1... | collective-permute-start | bytes 1572872 | tf_op jit(solution)/shard_map/ppermute | solution.py:207
  168.2 1.1 convolution_convert_fusion.1
  169.3 5.1 %all-to-all-start.2 = ((bf16[4,32,2048]{2,1,0:T(8,128)(2,1)}), bf16[4,32,2048]{2,1,0:T(8,128)(2,1)S(1)}, u32[]{:S(2)}, u32[]{:S(2)}) async-start(bf16[4,32,2048]{2,1,0:T(8,128)(2,1)} %bitcast.10), calls=%async_computation.2 | async-start | bytes 1048576 | tf_op jit(solution)/shard_map/all_to_all | solution.py:351
  174.4 13.6 %collective-permute-done.12 = bf16[128,2048]{1,0:T(8,128)(2,1)} collective-permute-done((bf16[128,2048]{1,0:T(8,128)(2,1)S(1)}, bf16[128,2048]{1,0:T(8,128)(2,1)}, u32[]{:S(2)}, u32[]{:S(2)}) %collective-permute-start.12) | collective-permute-done | bytes 524320 | tf_op jit(solution)/shard_map/ppermute | solution.py:207
  188.1 1.4 add_convert_fusion.2
  189.6 1.4 add_convert_fusion
  191.7 2.1 pad_maximum_fusion.1
  193.8 13.3 %all-to-all-start.4 = ((bf16[64,4,2048]{2,1,0:T(4,128)(2,1)}), bf16[64,4,2048]{2,1,0:T(4,128)(2,1)S(1)}, u32[]{:S(2)}, u32[]{:S(2)}) async-start(bf16[64,4,2048]{2,1,0:T(4,128)(2,1)} %pad_maximum_fusion.1), calls=%async_computation.4 | async-start | bytes 2097152 | tf_op jit(solution)/shard_map/all_to_all | solution.py:303
  208.0 27.9 %all-to-all-done.4 = bf16[64,4,2048]{2,1,0:T(4,128)(2,1)S(1)} async-done(((bf16[64,4,2048]{2,1,0:T(4,128)(2,1)}), bf16[64,4,2048]{2,1,0:T(4,128)(2,1)S(1)}, u32[]{:S(2)}, u32[]{:S(2)}) %all-to-all-start.4) | async-done | bytes 1048608 | tf_op jit(solution)/shard_map/all_to_all | solution.py:303
  236.6 0.9 multiply_convert_fusion
  (85 shorter events, 6.9 us)
Async XLA Ops:
  0.6 167.6 %copy-start = (bf16[256,2048]{1,0:T(8,128)(2,1)S(1)}, bf16[256,2048]{1,0:T(8,128)(2,1)}, u32[]{:S(2)}) copy-start(bf16[256,2048]{1,0:T(8,128)(2,1)} %param.21) | copy-start | bytes 3145732
  2.5 19.5 %all-to-all-start = ((bf16[4,272,128]{2,1,0:T(8,128)(2,1)}), bf16[4,272,128]{2,1,0:T(8,128)(2,1)S(1)}, u32[]{:S(2)}, u32[]{:S(2)}) async-start(bf16[4,272,128]{2,1,0:T(8,128)(2,1)} %pack.1), calls=%async_computation | async-start | bytes 557056 | tf_op jit(solution)/shard_map/all_to_all | solution.py:306
  13.5 2.7 %copy-start.10 = (bf16[256,96]{0,1:T(8,128)(2,1)}, bf16[256,96]{0,1:T(8,128)(2,1)S(1)}, u32[]{:S(2)}) copy-start(bf16[256,96]{0,1:T(8,128)(2,1)S(1)} %fusion.14) | copy-start | bytes 147460
  23.8 68.5 %all-to-all-start.3 = ((bf16[64,4,2176]{2,1,0:T(4,128)(2,1)}), bf16[64,4,2176]{2,1,0:T(4,128)(2,1)S(1)}, u32[]{:S(2)}, u32[]{:S(2)}) async-start(bf16[64,4,2176]{2,1,0:T(4,128)(2,1)} %reshape.183), calls=%async_computation.3 | async-start | bytes 2228224 | tf_op jit(solution)/shard_map/all_to_all | solution.py:303
  30.5 29.2 %collective-permute-start = (bf16[528,128]{1,0:T(8,128)(2,1)S(1)}, bf16[528,128]{1,0:T(8,128)(2,1)S(1)}, u32[]{:S(2)}, u32[]{:S(2)}) collective-permute-start(bf16[528,128]{1,0:T(8,128)(2,1)S(1)} %get-tuple-element.23), channel_id=1, source_target_pairs={{0,32},{4,36},{8,40},{12,44},{16,48},{20,52},{24,56},{28,60},{32,0... | collective-permute-start | bytes 405512 | tf_op jit(solution)/shard_map/ppermute | solution.py:314
  59.7 19.4 %copy-start.3 = (bf16[2,528,128]{2,1,0:T(8,128)(2,1)}, bf16[2,528,128]{2,1,0:T(8,128)(2,1)S(1)}, u32[]{:S(2)}) copy-start(bf16[2,528,128]{2,1,0:T(8,128)(2,1)S(1)} %pad_maximum_fusion.2.refs_0_) | copy-start | bytes 811012
  59.7 14.0 %collective-permute-start.1 = (bf16[2,528,128]{2,1,0:T(8,128)(2,1)S(1)}, bf16[2,528,128]{2,1,0:T(8,128)(2,1)S(1)}, u32[]{:S(2)}, u32[]{:S(2)}) collective-permute-start(bf16[2,528,128]{2,1,0:T(8,128)(2,1)S(1)} %pad_maximum_fusion.2.refs_0_), channel_id=1, source_target_pairs={{0,24},{4,28},{8,0},{12,4},{16,8},{20,12},{24,16},{28,20},{32,56},... | collective-permute-start | bytes 811016 | tf_op jit(solution)/shard_map/ppermute | solution.py:314
  62.5 11.3 %collective-permute-start.2 = (bf16[2,528,128]{2,1,0:T(8,128)(2,1)S(1)}, bf16[2,528,128]{2,1,0:T(8,128)(2,1)S(1)}, u32[]{:S(2)}, u32[]{:S(2)}) collective-permute-start(bf16[2,528,128]{2,1,0:T(8,128)(2,1)S(1)} %pad_maximum_fusion.2.refs_0_), channel_id=1, source_target_pairs={{0,16},{4,20},{8,24},{12,28},{16,0},{20,4},{24,8},{28,12},{32,48},... | collective-permute-start | bytes 811016 | tf_op jit(solution)/shard_map/ppermute | solution.py:314
  63.3 14.1 %collective-permute-start.3 = (bf16[2,528,128]{2,1,0:T(8,128)(2,1)S(1)}, bf16[2,528,128]{2,1,0:T(8,128)(2,1)S(1)}, u32[]{:S(2)}, u32[]{:S(2)}) collective-permute-start(bf16[2,528,128]{2,1,0:T(8,128)(2,1)S(1)} %pad_maximum_fusion.2.refs_0_), channel_id=1, source_target_pairs={{0,8},{4,12},{8,16},{12,20},{16,24},{20,28},{24,0},{28,4},{32,40},... | collective-permute-start | bytes 811016 | tf_op jit(solution)/shard_map/ppermute | solution.py:314
  64.2 13.3 %collective-permute-start.4 = (bf16[2,528,128]{2,1,0:T(8,128)(2,1)S(1)}, bf16[2,528,128]{2,1,0:T(8,128)(2,1)S(1)}, u32[]{:S(2)}, u32[]{:S(2)}) collective-permute-start(bf16[2,528,128]{2,1,0:T(8,128)(2,1)S(1)} %pad_maximum_fusion.2.refs_0_), channel_id=1, source_target_pairs={{0,4},{4,0},{8,12},{12,8},{16,20},{20,16},{24,28},{28,24},{32,36},... | collective-permute-start | bytes 811016 | tf_op jit(solution)/shard_map/ppermute | solution.py:314
  73.7 5.4 %copy-start.12 = (bf16[2,528,128]{2,1,0:T(8,128)(2,1)}, bf16[2,528,128]{2,1,0:T(8,128)(2,1)S(1)}, u32[]{:S(2)}) copy-start(bf16[2,528,128]{2,1,0:T(8,128)(2,1)S(1)} %collective-permute-done.1.refs_1_) | copy-start | bytes 811012
  73.7 3.7 %collective-permute-start.5 = (bf16[2,528,128]{2,1,0:T(8,128)(2,1)S(1)}, bf16[2,528,128]{2,1,0:T(8,128)(2,1)}, u32[]{:S(2)}, u32[]{:S(2)}) collective-permute-start(bf16[2,528,128]{2,1,0:T(8,128)(2,1)S(1)} %collective-permute-done.1.refs_1_), channel_id=1, source_target_pairs={{0,4},{4,0},{8,12},{12,8},{16,20},{20,16},{24,28},{28,24},{32,36},... | collective-permute-start | bytes 811016 | tf_op jit(solution)/shard_map/ppermute | solution.py:314
  73.7 5.4 %copy-start.13 = (bf16[2,528,128]{2,1,0:T(8,128)(2,1)}, bf16[2,528,128]{2,1,0:T(8,128)(2,1)S(1)}, u32[]{:S(2)}) copy-start(bf16[2,528,128]{2,1,0:T(8,128)(2,1)S(1)} %collective-permute-done.2.refs_2_) | copy-start | bytes 811012
  73.8 3.7 %collective-permute-start.6 = (bf16[2,528,128]{2,1,0:T(8,128)(2,1)S(1)}, bf16[2,528,128]{2,1,0:T(8,128)(2,1)}, u32[]{:S(2)}, u32[]{:S(2)}) collective-permute-start(bf16[2,528,128]{2,1,0:T(8,128)(2,1)S(1)} %collective-permute-done.2.refs_2_), channel_id=1, source_target_pairs={{0,4},{4,0},{8,12},{12,8},{16,20},{20,16},{24,28},{28,24},{32,36},... | collective-permute-start | bytes 811016 | tf_op jit(solution)/shard_map/ppermute | solution.py:314
  77.4 1.7 copy-start.14
  77.4 1.7 collective-permute-start.7
  77.4 1.7 copy-start.15
  93.3 36.3 %copy-start.2 = (bf16[128,2176]{1,0:T(8,128)(2,1)}, bf16[128,2176]{1,0:T(8,128)(2,1)S(1)}, u32[]{:S(2)}) copy-start(bf16[128,2176]{1,0:T(8,128)(2,1)S(1)} %reshape.184.refs_0_) | copy-start | bytes 1671172
  93.3 14.8 %collective-permute-start.8 = (bf16[128,2176]{1,0:T(8,128)(2,1)S(1)}, bf16[128,2176]{1,0:T(8,128)(2,1)}, u32[]{:S(2)}, u32[]{:S(2)}) collective-permute-start(bf16[128,2176]{1,0:T(8,128)(2,1)S(1)} %reshape.184.refs_0_), channel_id=1, source_target_pairs={{0,1},{1,2},{2,3},{3,0},{4,5},{5,6},{6,7},{7,4},{8,9},{9,10},{10,1... | collective-permute-start | bytes 1671176 | tf_op jit(solution)/shard_map/ppermute | solution.py:207
  94.1 35.5 %copy-start.1 = (bf16[128,2176]{1,0:T(8,128)(2,1)}, bf16[128,2176]{1,0:T(8,128)(2,1)S(1)}, u32[]{:S(2)}) copy-start(bf16[128,2176]{1,0:T(8,128)(2,1)S(1)} %reshape.186.refs_0_) | copy-start | bytes 1671172
  94.1 15.8 %collective-permute-start.15 = (bf16[128,2176]{1,0:T(8,128)(2,1)S(1)}, bf16[128,2176]{1,0:T(8,128)(2,1)}, u32[]{:S(2)}, u32[]{:S(2)}) collective-permute-start(bf16[128,2176]{1,0:T(8,128)(2,1)S(1)} %reshape.186.refs_0_), channel_id=1, source_target_pairs={{0,3},{1,0},{2,1},{3,2},{4,7},{5,4},{6,5},{7,6},{8,11},{9,8},{10,9... | collective-permute-start | bytes 1671176 | tf_op jit(solution)/shard_map/ppermute | solution.py:207
  108.2 15.7 %collective-permute-start.10 = (bf16[128,2176]{1,0:T(8,128)(2,1)}, bf16[128,2176]{1,0:T(8,128)(2,1)S(1)}, u32[]{:S(2)}, u32[]{:S(2)}) collective-permute-start(bf16[128,2176]{1,0:T(8,128)(2,1)} %collective-permute-done.8.refs_1_), channel_id=1, source_target_pairs={{0,1},{1,2},{2,3},{3,0},{4,5},{5,6},{6,7},{7,4},{8,9},{9,10},{10,1... | collective-permute-start | bytes 1671176 | tf_op jit(solution)/shard_map/ppermute | solution.py:207
  109.9 20.7 %collective-permute-start.17 = (bf16[128,2176]{1,0:T(8,128)(2,1)}, bf16[128,2176]{1,0:T(8,128)(2,1)S(1)}, u32[]{:S(2)}, u32[]{:S(2)}) collective-permute-start(bf16[128,2176]{1,0:T(8,128)(2,1)} %collective-permute-done.15.refs_2_), channel_id=1, source_target_pairs={{0,3},{1,0},{2,1},{3,2},{4,7},{5,4},{6,5},{7,6},{8,11},{9,8},{10,9... | collective-permute-start | bytes 1671176 | tf_op jit(solution)/shard_map/ppermute | solution.py:207
  110.2 37.1 %collective-permute-start.9 = (bf16[128,2176]{1,0:T(8,128)(2,1)S(1)}, bf16[128,2176]{1,0:T(8,128)(2,1)}, u32[]{:S(2)}, u32[]{:S(2)}) collective-permute-start(bf16[128,2176]{1,0:T(8,128)(2,1)S(1)} %reshape.184.refs_0_), channel_id=1, source_target_pairs={{0,3},{1,0},{2,1},{3,2},{4,7},{5,4},{6,5},{7,6},{8,11},{9,8},{10,9... | collective-permute-start | bytes 1671176 | tf_op jit(solution)/shard_map/ppermute | solution.py:207
  111.0 45.0 %collective-permute-start.14 = (bf16[128,2176]{1,0:T(8,128)(2,1)S(1)}, bf16[128,2176]{1,0:T(8,128)(2,1)}, u32[]{:S(2)}, u32[]{:S(2)}) collective-permute-start(bf16[128,2176]{1,0:T(8,128)(2,1)S(1)} %reshape.186.refs_0_), channel_id=1, source_target_pairs={{0,1},{1,2},{2,3},{3,0},{4,5},{5,6},{6,7},{7,4},{8,9},{9,10},{10,1... | collective-permute-start | bytes 1671176 | tf_op jit(solution)/shard_map/ppermute | solution.py:207
  123.9 0.8 copy-start.6
  129.6 9.0 %copy-start.4 = (f32[512,128]{1,0:T(8,128)S(1)}, f32[512,128]{1,0:T(8,128)}, u32[]{:S(2)}) copy-start(f32[512,128]{1,0:T(8,128)} %attend.1) | copy-start | bytes 786436
  129.6 33.8 %collective-permute-start.11 = (bf16[128,2048]{1,0:T(8,128)(2,1)}, bf16[128,2048]{1,0:T(8,128)(2,1)S(1)}, u32[]{:S(2)}, u32[]{:S(2)}) collective-permute-start(bf16[128,2048]{1,0:T(8,128)(2,1)} %expert_layer.5), channel_id=1, source_target_pairs={{0,3},{1,0},{2,1},{3,2},{4,7},{5,4},{6,5},{7,6},{8,11},{9,8},{10,9... | collective-permute-start | bytes 1572872 | tf_op jit(solution)/shard_map/ppermute | solution.py:207
  130.5 0.8 copy-start.5
  136.2 27.4 %collective-permute-start.18 = (bf16[128,2048]{1,0:T(8,128)(2,1)}, bf16[128,2048]{1,0:T(8,128)(2,1)S(1)}, u32[]{:S(2)}, u32[]{:S(2)}) collective-permute-start(bf16[128,2048]{1,0:T(8,128)(2,1)} %expert_layer.7), channel_id=1, source_target_pairs={{0,1},{1,2},{2,3},{3,0},{4,5},{5,6},{6,7},{7,4},{8,9},{9,10},{10,1... | collective-permute-start | bytes 1572872 | tf_op jit(solution)/shard_map/ppermute | solution.py:207
  141.0 27.1 %all-to-all-start.1 = ((bf16[4,128,64]{1,2,0:T(8,128)(2,1)}), bf16[4,128,64]{1,2,0:T(8,128)(2,1)S(1)}, u32[]{:S(2)}, u32[]{:S(2)}) async-start(bf16[4,128,64]{1,2,0:T(8,128)(2,1)} %copy.30), calls=%async_computation.1 | async-start | bytes 131072 | tf_op jit(solution)/shard_map/all_to_all | solution.py:348
  154.3 9.1 %copy-start.7 = (bf16[128,2048]{1,0:T(8,128)(2,1)S(1)}, bf16[128,2048]{1,0:T(8,128)(2,1)}, u32[]{:S(2)}) copy-start(bf16[128,2048]{1,0:T(8,128)(2,1)} %get-tuple-element.13) | copy-start | bytes 1572868
  154.3 20.1 %collective-permute-start.13 = (bf16[128,2048]{1,0:T(8,128)(2,1)}, bf16[128,2048]{1,0:T(8,128)(2,1)}, u32[]{:S(2)}, u32[]{:S(2)}) collective-permute-start(bf16[128,2048]{1,0:T(8,128)(2,1)} %get-tuple-element.14), channel_id=1, source_target_pairs={{0,1},{1,2},{2,3},{3,0},{4,5},{5,6},{6,7},{7,4},{8,9},{9,10},{10,1... | collective-permute-start | bytes 1572872 | tf_op jit(solution)/shard_map/ppermute | solution.py:207
  163.1 26.5 %collective-permute-start.16 = (bf16[128,2048]{1,0:T(8,128)(2,1)}, bf16[128,2048]{1,0:T(8,128)(2,1)}, u32[]{:S(2)}, u32[]{:S(2)}) collective-permute-start(bf16[128,2048]{1,0:T(8,128)(2,1)} %get-tuple-element.16), channel_id=1, source_target_pairs={{0,3},{1,0},{2,1},{3,2},{4,7},{5,4},{6,5},{7,6},{8,11},{9,8},{10,9... | collective-permute-start | bytes 1572872 | tf_op jit(solution)/shard_map/ppermute | solution.py:207
  163.6 24.5 %collective-permute-start.12 = (bf16[128,2048]{1,0:T(8,128)(2,1)S(1)}, bf16[128,2048]{1,0:T(8,128)(2,1)}, u32[]{:S(2)}, u32[]{:S(2)}) collective-permute-start(bf16[128,2048]{1,0:T(8,128)(2,1)S(1)} %add_convert_fusion.3), channel_id=1, source_target_pairs={{0,3},{1,0},{2,1},{3,2},{4,7},{5,4},{6,5},{7,6},{8,11},{9,8},{10,9... | collective-permute-start | bytes 1572872 | tf_op jit(solution)/shard_map/ppermute | solution.py:207
  163.7 24.4 %copy-start.8 = (bf16[128,2048]{1,0:T(8,128)(2,1)S(1)}, bf16[128,2048]{1,0:T(8,128)(2,1)}, u32[]{:S(2)}) copy-start(bf16[128,2048]{1,0:T(8,128)(2,1)} %get-tuple-element.12) | copy-start | bytes 1572868
  164.9 24.6 %collective-permute-start.19 = (bf16[128,2048]{1,0:T(8,128)(2,1)S(1)}, bf16[128,2048]{1,0:T(8,128)(2,1)}, u32[]{:S(2)}, u32[]{:S(2)}) collective-permute-start(bf16[128,2048]{1,0:T(8,128)(2,1)S(1)} %add_convert_fusion.1), channel_id=1, source_target_pairs={{0,1},{1,2},{2,3},{3,0},{4,5},{5,6},{6,7},{7,4},{8,9},{9,10},{10,1... | collective-permute-start | bytes 1572872 | tf_op jit(solution)/shard_map/ppermute | solution.py:207
  169.3 24.4 %all-to-all-start.2 = ((bf16[4,32,2048]{2,1,0:T(8,128)(2,1)}), bf16[4,32,2048]{2,1,0:T(8,128)(2,1)S(1)}, u32[]{:S(2)}, u32[]{:S(2)}) async-start(bf16[4,32,2048]{2,1,0:T(8,128)(2,1)} %bitcast.10), calls=%async_computation.2 | async-start | bytes 1048576 | tf_op jit(solution)/shard_map/all_to_all | solution.py:351
  174.4 15.1 %copy-start.9 = (bf16[128,2048]{1,0:T(8,128)(2,1)S(1)}, bf16[128,2048]{1,0:T(8,128)(2,1)}, u32[]{:S(2)}) copy-start(bf16[128,2048]{1,0:T(8,128)(2,1)} %get-tuple-element.15) | copy-start | bytes 1572868
  193.8 13.5 %copy-start.17 = (f32[2048]{0:T(1024)S(1)}, f32[2048]{0:T(1024)}, u32[]{:S(2)}) copy-start(f32[2048]{0:T(1024)} %param.22) | copy-start | bytes 24580
  193.8 42.1 %all-to-all-start.4 = ((bf16[64,4,2048]{2,1,0:T(4,128)(2,1)}), bf16[64,4,2048]{2,1,0:T(4,128)(2,1)S(1)}, u32[]{:S(2)}, u32[]{:S(2)}) async-start(bf16[64,4,2048]{2,1,0:T(4,128)(2,1)} %pad_maximum_fusion.1), calls=%async_computation.4 | async-start | bytes 2097152 | tf_op jit(solution)/shard_map/all_to_all | solution.py:303
  207.0 29.1 %copy-start.11 = (bf16[256,96]{0,1:T(8,128)(2,1)S(1)}, bf16[256,96]{0,1:T(8,128)(2,1)}, u32[]{:S(2)}) copy-start(bf16[256,96]{0,1:T(8,128)(2,1)} %copy-done.10) | copy-start | bytes 147460
  207.3 29.3 %copy-start.16 = (f32[2048]{0:T(1024)S(1)}, f32[2048]{0:T(1024)}, u32[]{:S(2)}) copy-start(f32[2048]{0:T(1024)} %param.33) | copy-start | bytes 24580
